TPU v7x, 32 devices: a whole 2x2x4 slice. The times are simulated.
32 devices in a mesh: fs: 8 (over z, y), tp: 4 (over x, core).
Axes of the slice: x: 2, y: 2, z: 4, core: 2. Of those that a mesh axis runs over, the one named last changes fastest.
Arguments:
- tokens: bfloat16 [2048, 2048], P('fs', 'tp'), may hold values from -12.1 to 12.1, as said below
- gate_weight: float32 [2048, 5632], P('fs', 'tp'), may hold values from -0.125 to 0.125
- up_weight: float32 [2048, 5632], P('fs', 'tp'), may hold values from -0.125 to 0.125
- down_weight: float32 [5632, 2048], P('tp', 'fs'), may hold values from -0.078125 to 0.078125
- gate_scale: float32 [4, 1408], P('tp', 'fs'), may hold values from 0.1 to 1.9
- up_scale: float32 [4, 1408], P('tp', 'fs'), may hold values from 0.1 to 1.9
- down_scale: float32 [4, 512], P('tp', 'fs'), may hold values from 0.16 to 4.6, as said below
- bgate_weight: float32 [2048, 2048], P('fs', 'tp'), may hold values from -0.125 to 0.125
- cgate_weight: float32 [2048, 2048], P('fs', 'tp'), may hold values from -0.125 to 0.125
- value_weight: float32 [2048, 2048], P('fs', 'tp'), may hold values from -0.125 to 0.125
- bgate_scale: float32 [4, 512], P('tp', 'fs'), may hold values from 0.1 to 1.9
- cgate_scale: float32 [4, 512], P('tp', 'fs'), may hold values from 0.1 to 1.9
- value_scale: float32 [4, 512], P('tp', 'fs'), may hold values from 0.1 to 1.9
- conv_taps: float32 [3, 2048], replicated, may hold values from -3.5 to 3.5
- mixout_weight: float32 [2048, 2048], P('tp', 'fs'), may hold values from -0.125 to 0.125
- mixout_scale: float32 [4, 512], P('tp', 'fs'), may hold values from 0.16 to 4.6, as said below
- first_gain: float32 [2048], replicated, may hold values from 0.1 to 1.9
- first_shift: float32 [2048], replicated, may hold values from -1.8 to 1.8
- mixer_gain: float32 [2048], replicated, may hold values from 0.1 to 1.9
- mixer_shift: float32 [2048], replicated, may hold values from -1.8 to 1.8
- last_gain: float32 [2048], replicated, may hold values from 0.1 to 1.9
- last_shift: float32 [2048], replicated, may hold values from -1.8 to 1.8
Outputs:
- layer_out: bfloat16 [2048, 2048], P('fs', 'tp')
Inputs may be any that keep to these rules, and one draw needn't show every extreme that they name: `tokens`: normal values times one factor for each of 4 equal consecutive blocks of the features. `down_scale`: positive; one factor for each row times a spread over the columns. `mixout_scale`: positive; one factor for each row times a spread over the columns.
All inputs are finite; a program needn't handle non-finite values.
Results may differ from a plain program's by a relative error of at most 0.025.
Values may be sent and summed in bfloat16 or wider, within the bound.
No kernel may reach another device: no remote copies, remote signals or barrier semaphores. Data moves between devices by JAX's collectives and lax.ppermute only.
A program may use at most 64 MiB of HBM per device.

v0:
```python
import jax
import jax.numpy as jnp
from jax import lax
from jax.sharding import PartitionSpec as P

TAPS = 3
LENGTH = 128
RESIDUAL_SCALE = 1.4142135623730951
HALF_STEP = 0.5
EPSILON = 1e-05


def add_rows(gathered, shard_piece):
    return jnp.dot(gathered, shard_piece, preferred_element_type=jnp.float32)


def features(inputs):
    return lax.all_gather(inputs, "tp", axis=1, tiled=True)


def post_norm(residual, branch, norm_gain, norm_shift):
    summed = RESIDUAL_SCALE * residual.astype(jnp.float32) + branch
    moments = lax.psum((jnp.sum(summed, -1), jnp.sum(summed * summed, -1)), "tp")
    feature_total = summed.shape[1] * lax.axis_size("tp")
    average = (moments[0] / feature_total)[:, None]
    mean_square = (moments[1] / feature_total)[:, None]
    variance = mean_square - average * average
    return ((summed - average) * lax.rsqrt(variance + EPSILON) * norm_gain + norm_shift).astype(
        jnp.bfloat16
    )


def spread_back(weight_cols, left_rows):
    return (
        lax.psum_scatter(
            lax.dot_general(
                weight_cols, left_rows, (((0,), (1,)), ((), ())), preferred_element_type=jnp.float32
            ).astype(jnp.bfloat16),
            "tp",
            scatter_dimension=0,
            tiled=True,
        )
        .astype(jnp.float32)
        .T
    )


def shards(
    tokens,
    gate_weight,
    up_weight,
    down_weight,
    gate_scale,
    up_scale,
    down_scale,
    bgate_weight,
    cgate_weight,
    value_weight,
    bgate_scale,
    cgate_scale,
    value_scale,
    conv_taps,
    mixout_weight,
    mixout_scale,
    first_gain,
    first_shift,
    mixer_gain,
    mixer_shift,
    last_gain,
    last_shift,
):
    scales = (
        lax.all_gather(gate_scale, "fs", axis=1, tiled=True),
        lax.all_gather(up_scale, "fs", axis=1, tiled=True),
        lax.all_gather(down_scale, "fs", axis=1, tiled=True),
        lax.all_gather(bgate_scale, "fs", axis=1, tiled=True),
        lax.all_gather(cgate_scale, "fs", axis=1, tiled=True),
        lax.all_gather(value_scale, "fs", axis=1, tiled=True),
        lax.all_gather(mixout_scale, "fs", axis=1, tiled=True),
    )
    gate_cols, up_cols, down_cols, bgate_cols, cgate_cols, value_cols, mixout_cols = [
        scale_row.reshape(-1) for scale_row in scales
    ]
    tp_index = lax.axis_index("tp")
    columns = tokens.shape[1]

    def own_part(vector):
        return lax.dynamic_slice_in_dim(vector, tp_index * columns, columns)

    gate_low = gate_weight.astype(jnp.bfloat16)
    up_low = up_weight.astype(jnp.bfloat16)
    down_low = down_weight.astype(jnp.bfloat16)
    kept_gate, kept_up = (
        lax.all_gather(gate_low, "fs", axis=0, tiled=True),
        lax.all_gather(up_low, "fs", axis=0, tiled=True),
    )
    kept_down = lax.all_gather(down_low, "fs", axis=1, tiled=True)

    def channel_mix(gathered):
        gate_sum = jnp.dot(gathered, kept_gate, preferred_element_type=jnp.float32)
        up_sum = jnp.dot(gathered, kept_up, preferred_element_type=jnp.float32)
        hidden = (jax.nn.silu(gate_sum * gate_cols) * (up_sum * up_cols)).astype(jnp.bfloat16)
        return HALF_STEP * (spread_back(kept_down, hidden) * down_cols)

    first = post_norm(
        tokens, channel_mix(features(tokens)), own_part(first_gain), own_part(first_shift)
    )
    gathered = features(first)
    bgate_low = bgate_weight.astype(jnp.bfloat16)
    channels = bgate_low.shape[1]
    outgate = add_rows(gathered, lax.all_gather(bgate_low, "fs", axis=0, tiled=True))
    ingate = add_rows(
        gathered, lax.all_gather(cgate_weight.astype(jnp.bfloat16), "fs", axis=0, tiled=True)
    )
    values = add_rows(
        gathered, lax.all_gather(value_weight.astype(jnp.bfloat16), "fs", axis=0, tiled=True)
    )
    tap_weights = lax.dynamic_slice_in_dim(conv_taps, tp_index * channels, channels, 1)
    mixed = (ingate * cgate_cols * (values * value_cols)).reshape(-1, LENGTH, channels)
    padded = jnp.pad(mixed, ((0, 0), (TAPS - 1, 0), (0, 0)))
    convolved = jnp.zeros(mixed.shape, jnp.float32)
    for tap_index in range(TAPS):
        convolved = convolved + tap_weights[tap_index] * padded[:, tap_index : tap_index + LENGTH]
    gated = (outgate * bgate_cols * convolved.reshape(-1, channels)).astype(jnp.bfloat16)
    mix_full = lax.all_gather(mixout_weight.astype(jnp.bfloat16), "fs", axis=1, tiled=True)
    second = post_norm(
        first,
        spread_back(mix_full, gated) * mixout_cols,
        own_part(mixer_gain),
        own_part(mixer_shift),
    )
    return post_norm(
        second, channel_mix(features(second)), own_part(last_gain), own_part(last_shift)
    )


def solution(mesh):
    in_specs = (
        P("fs", "tp"),
        P("fs", "tp"),
        P("fs", "tp"),
        P("tp", "fs"),
        P("tp", "fs"),
        P("tp", "fs"),
        P("tp", "fs"),
        P("fs", "tp"),
        P("fs", "tp"),
        P("fs", "tp"),
        P("tp", "fs"),
        P("tp", "fs"),
        P("tp", "fs"),
        P(),
        P("tp", "fs"),
        P("tp", "fs"),
        P(),
        P(),
        P(),
        P(),
        P(),
        P(),
    )
    out_specs = P("fs", "tp")
    return jax.shard_map(shards, mesh=mesh, in_specs=in_specs, out_specs=out_specs, check_vma=False)
```

profile of v0, /device:TPU:0, one launch (start us, length us, event | category | flops | bytes accessed | tf_op | source)
XLA Modules:
  0.0 669.1 jit_solution(10766681198082173955)
XLA Ops:
  7.3 2.3 convert_element_type.78
  15.2 39.5 %all-reduce.8 = (f32[1408]{0:T(1024)S(1)}, f32[1408]{0:T(1024)S(1)}, f32[512]{0:T(512)S(1)}, f32[512]{0:T(512)S(1)}, f32[512]{0:T(512)S(1)}, /*index=5*/f32[512]{0:T(512)S(1)}, f32[512]{0:T(512)S(1)}) all-reduce(f32[1408]{0:T(1024)S(1)} %dynamic-update-slice, f32[1408]{0:T(1024)S(1)} %dynamic-update-slice.1, ...), channel_id=1, replica_groups=mesh['fs'=8,'tp'=4] {'fs'}, use_global_device_ids=true, to_apply=%add.1 | all-reduce | flops 5376 | bytes 43008
  54.7 68.3 %all-gather.13.cloned.1.call-done = bf16[2048,1408]{1,0:T(8,128)(2,1)} async-done(((bf16[256,1408]{1,0:T(8,128)(2,1)}), bf16[2048,1408]{1,0:T(8,128)(2,1)}) %all-gather.13.cloned.1.call-update) | async-done | bytes 5767184 | tf_op jit(solution)/shard_map/all_gather | solution.py:94
  123.1 4.8 convolution_multiply_fusion.3
  127.9 87.9 %all-gather.15.cloned.1.call-done = bf16[2048,1408]{1,0:T(8,128)(2,1)} async-done(((bf16[256,1408]{1,0:T(8,128)(2,1)}), bf16[2048,1408]{1,0:T(8,128)(2,1)}) %all-gather.15.cloned.1.call-update) | async-done | bytes 5767184 | tf_op jit(solution)/shard_map/all_gather | solution.py:95
  215.8 93.2 %all-gather.17.cloned.1.call-done = bf16[1408,2048]{1,0:T(8,128)(2,1)} async-done(((bf16[1408,256]{1,0:T(8,128)(2,1)}), bf16[1408,2048]{1,0:T(8,128)(2,1)}) %all-gather.17.cloned.1.call-update) | async-done | bytes 5767184 | tf_op jit(solution)/shard_map/all_gather | solution.py:97
  309.0 9.0 %fusion.4 = bf16[2048,256]{0,1:T(8,128)(2,1)} fusion(bf16[1408,2048]{1,0:T(8,128)(2,1)} %all-gather.17.cloned.1.call-done, bf16[256,2048]{1,0:T(8,128)(2,1)S(1)} %copy-done.12, bf16[2048,1408]{1,0:T(8,128)(2,1)} %all-gather.15.cloned.1.call-done, f32[256,1408]{1,0:T(8,128)S(1)} %convolution_multiply_fusion.3, f32[1408]{0:T(1024)S(1)} %get-tuple-element.12), kind=kOutput, calls=%fused_computation.11 | convolution fusion | flops 2955837440 | bytes 15078912 | tf_op jit(solution)/shard_map/dot_general | solution.py:36
  320.5 20.6 %reduce-scatter.4.cloned.1.call-done = bf16[512,256]{0,1:T(8,128)(2,1)} async-done(((bf16[2048,256]{0,1:T(8,128)(2,1)}), bf16[512,256]{0,1:T(8,128)(2,1)}) %reduce-scatter.4.cloned.1.call-update) | async-done | bytes 262160 | tf_op jit(solution)/shard_map/reduce_scatter | solution.py:35
  342.3 5.8 all-reduce.11
  353.4 38.9 %all-gather.23.cloned.1.call-done = bf16[2048,512]{1,0:T(8,128)(2,1)} async-done(((bf16[256,512]{1,0:T(8,128)(2,1)}), bf16[2048,512]{1,0:T(8,128)(2,1)}) %all-gather.23.cloned.1.call-update) | async-done | bytes 2097168 | tf_op jit(solution)/shard_map/all_gather | solution.py:113
  392.2 16.8 %all-gather.19.cloned.1.call-done = bf16[256,2048]{1,0:T(8,128)(2,1)} async-done(((bf16[256,512]{1,0:T(8,128)(2,1)}), bf16[256,2048]{1,0:T(8,128)(2,1)}) %all-gather.19.cloned.1.call-update) | async-done | bytes 1048592 | tf_op jit(solution)/shard_map/all_gather | solution.py:18
  409.0 2.7 convolution_multiply_fusion.5
  411.8 48.5 %all-gather.25.cloned.1.call-done = bf16[2048,512]{1,0:T(8,128)(2,1)} async-done(((bf16[256,512]{1,0:T(8,128)(2,1)}), bf16[2048,512]{1,0:T(8,128)(2,1)}) %all-gather.25.cloned.1.call-update) | async-done | bytes 2097168 | tf_op jit(solution)/shard_map/all_gather | solution.py:116
  460.3 2.3 fusion.7
  462.8 47.3 %all-gather.21.cloned.1.call-done = bf16[2048,512]{1,0:T(8,128)(2,1)} async-done(((bf16[256,512]{1,0:T(8,128)(2,1)}), bf16[2048,512]{1,0:T(8,128)(2,1)}) %all-gather.21.cloned.1.call-update) | async-done | bytes 2097168 | tf_op jit(solution)/shard_map/all_gather | solution.py:111
  510.1 50.8 %all-gather.27.cloned.1.call-done = bf16[512,2048]{1,0:T(8,128)(2,1)} async-done(((bf16[512,256]{1,0:T(8,128)(2,1)}), bf16[512,2048]{1,0:T(8,128)(2,1)}) %all-gather.27.cloned.1.call-update) | async-done | bytes 2097168 | tf_op jit(solution)/shard_map/all_gather | solution.py:125
  560.9 4.7 fusion.6
  567.1 21.6 %reduce-scatter.6.cloned.1.call-done = bf16[512,256]{0,1:T(8,128)(2,1)} async-done(((bf16[2048,256]{0,1:T(8,128)(2,1)}), bf16[512,256]{0,1:T(8,128)(2,1)}) %reduce-scatter.6.cloned.1.call-update) | async-done | bytes 262160 | tf_op jit(solution)/shard_map/reduce_scatter | solution.py:35
  589.9 5.8 all-reduce.10
  597.7 17.2 %all-gather.29.cloned.1.call-done = bf16[256,2048]{1,0:T(8,128)(2,1)} async-done(((bf16[256,512]{1,0:T(8,128)(2,1)}), bf16[256,2048]{1,0:T(8,128)(2,1)}) %all-gather.29.cloned.1.call-update) | async-done | bytes 1048592 | tf_op jit(solution)/shard_map/all_gather | solution.py:18
  615.0 4.8 convolution_multiply_fusion.1
  619.8 9.0 %fusion.5 = bf16[2048,256]{0,1:T(8,128)(2,1)} fusion(bf16[1408,2048]{1,0:T(8,128)(2,1)} %all-gather.17.cloned.1.call-done, bf16[256,2048]{1,0:T(8,128)(2,1)S(1)} %copy-done.13, bf16[2048,1408]{1,0:T(8,128)(2,1)} %all-gather.15.cloned.1.call-done, f32[256,1408]{1,0:T(8,128)S(1)} %convolution_multiply_fusion.1, f32[1408]{0:T(1024)S(1)} %get-tuple-element.12), kind=kOutput, calls=%fused_computation.12 | convolution fusion | flops 2955837440 | bytes 15078912 | tf_op jit(solution)/shard_map/dot_general | solution.py:36
  630.4 23.4 %reduce-scatter.8.cloned.1.call-done = bf16[512,256]{0,1:T(8,128)(2,1)} async-done(((bf16[2048,256]{0,1:T(8,128)(2,1)}), bf16[512,256]{0,1:T(8,128)(2,1)}) %reduce-scatter.8.cloned.1.call-update) | async-done | bytes 262160 | tf_op jit(solution)/shard_map/reduce_scatter | solution.py:35
  655.0 5.8 all-reduce.9
  (105 shorter events, 23.4 us)
Async XLA Ops:
  6.5 48.2 %all-gather.11.cloned.1.call-start = ((), (), s32[]{:S(2)}) async-start(), calls=%async_computation.3 | async-start | bytes 1310720 | tf_op jit(solution)/shard_map/all_gather | solution.py:18
  7.3 115.8 %all-gather.13.cloned.1.call-start = ((), (), s32[]{:S(2)}) async-start(), calls=%async_computation.4 | async-start | bytes 6488064 | tf_op jit(solution)/shard_map/all_gather | solution.py:94
  9.6 206.1 %all-gather.15.cloned.1.call-start = ((), (), s32[]{:S(2)}) async-start(), calls=%async_computation.5 | async-start | bytes 6488064 | tf_op jit(solution)/shard_map/all_gather | solution.py:95
  10.7 4.4 copy-start.18
  10.7 298.3 %all-gather.17.cloned.1.call-start = ((), (), s32[]{:S(2)}) async-start(), calls=%async_computation.6 | async-start | bytes 6488064 | tf_op jit(solution)/shard_map/all_gather | solution.py:97
  12.2 328.9 %reduce-scatter.4.cloned.1.call-start = ((), (), s32[]{:S(2)}) async-start(), calls=%async_computation.7 | async-start | bytes 1310720 | tf_op jit(solution)/shard_map/reduce_scatter | solution.py:35
  123.0 186.0 %copy-start.12 = (bf16[256,2048]{1,0:T(8,128)(2,1)S(1)}, bf16[256,2048]{1,0:T(8,128)(2,1)}, u32[]{:S(2)}) copy-start(bf16[256,2048]{1,0:T(8,128)(2,1)} %all-gather.11.cloned.1.call-done) | copy-start | bytes 3145732
  309.0 9.1 %copy-start.6 = (f32[256,512]{1,0:T(8,128)S(1)}, f32[256,512]{1,0:T(8,128)}, u32[]{:S(2)}) copy-start(f32[256,512]{1,0:T(8,128)} %param.30) | copy-start | bytes 1572868
  318.0 23.1 %copy-start.3 = (bf16[256,512]{1,0:T(8,128)(2,1)S(1)}, bf16[256,512]{1,0:T(8,128)(2,1)}, u32[]{:S(2)}) copy-start(bf16[256,512]{1,0:T(8,128)(2,1)} %param.22) | copy-start | bytes 786436
  318.0 32.0 %copy-start.7 = (f32[256,512]{1,0:T(8,128)S(1)}, f32[256,512]{1,0:T(8,128)}, u32[]{:S(2)}) copy-start(f32[256,512]{1,0:T(8,128)} %param.31) | copy-start | bytes 1572868
  318.0 32.8 %copy-start.8 = (f32[256,512]{1,0:T(8,128)S(1)}, f32[256,512]{1,0:T(8,128)}, u32[]{:S(2)}) copy-start(f32[256,512]{1,0:T(8,128)} %param.29) | copy-start | bytes 1572868
  318.0 74.2 %all-gather.23.cloned.1.call-start = ((), (), s32[]{:S(2)}) async-start(), calls=%async_computation.10 | async-start | bytes 2359296 | tf_op jit(solution)/shard_map/all_gather | solution.py:113
  318.8 32.8 %copy-start.9 = (f32[512,256]{1,0:T(8,128)S(1)}, f32[512,256]{1,0:T(8,128)}, u32[]{:S(2)}) copy-start(f32[512,256]{1,0:T(8,128)} %param.36) | copy-start | bytes 1572868
  318.8 90.2 %all-gather.19.cloned.1.call-start = ((), (), s32[]{:S(2)}) async-start(), calls=%async_computation.8 | async-start | bytes 1310720 | tf_op jit(solution)/shard_map/all_gather | solution.py:18
  350.0 110.3 %all-gather.25.cloned.1.call-start = ((), (), s32[]{:S(2)}) async-start(), calls=%async_computation.11 | async-start | bytes 2359296 | tf_op jit(solution)/shard_map/all_gather | solution.py:116
  350.8 159.3 %all-gather.21.cloned.1.call-start = ((), (), s32[]{:S(2)}) async-start(), calls=%async_computation.9 | async-start | bytes 2359296 | tf_op jit(solution)/shard_map/all_gather | solution.py:111
  351.6 209.3 %all-gather.27.cloned.1.call-start = ((), (), s32[]{:S(2)}) async-start(), calls=%async_computation.12 | async-start | bytes 2359296 | tf_op jit(solution)/shard_map/all_gather | solution.py:125
  352.4 236.3 %reduce-scatter.6.cloned.1.call-start = ((), (), s32[]{:S(2)}) async-start(), calls=%async_computation.13 | async-start | bytes 1310720 | tf_op jit(solution)/shard_map/reduce_scatter | solution.py:35
  409.0 51.2 %copy-start = (bf16[256,2048]{1,0:T(8,128)(2,1)S(1)}, bf16[256,2048]{1,0:T(8,128)(2,1)}, u32[]{:S(2)}) copy-start(bf16[256,2048]{1,0:T(8,128)(2,1)} %all-gather.19.cloned.1.call-done) | copy-start | bytes 3145732
  560.9 27.8 %copy-start.1 = (bf16[256,512]{1,0:T(8,128)(2,1)S(1)}, bf16[256,512]{1,0:T(8,128)(2,1)}, u32[]{:S(2)}) copy-start(bf16[256,512]{1,0:T(8,128)(2,1)} %add_convert_fusion.2) | copy-start | bytes 786436
  565.6 49.4 %all-gather.29.cloned.1.call-start = ((), (), s32[]{:S(2)}) async-start(), calls=%async_computation.14 | async-start | bytes 1310720 | tf_op jit(solution)/shard_map/all_gather | solution.py:18
  597.5 56.3 %reduce-scatter.8.cloned.1.call-start = ((), (), s32[]{:S(2)}) async-start(), calls=%async_computation.15 | async-start | bytes 1310720 | tf_op jit(solution)/shard_map/reduce_scatter | solution.py:35
  615.0 4.8 copy-start.13
  619.8 34.0 %copy-start.2 = (bf16[256,512]{1,0:T(8,128)(2,1)S(1)}, bf16[256,512]{1,0:T(8,128)(2,1)}, u32[]{:S(2)}) copy-start(bf16[256,512]{1,0:T(8,128)(2,1)} %add_convert_fusion.1) | copy-start | bytes 786436
  (9 other events, 30.6 us)
Sparse Core Ops, SparseCore 0:
  8.9 19.4 all-gather.10
  30.5 92.4 all-gather.12
  125.2 90.4 all-gather.14
  217.7 91.2 all-gather.16
  318.1 22.9 reduce-scatter.3
  343.1 49.1 all-gather.22
  393.8 15.2 all-gather.18
  411.2 49.0 all-gather.24
  462.4 47.6 all-gather.20
  512.0 48.8 all-gather.26
  565.7 22.9 reduce-scatter.5
  597.6 17.3 all-gather.28
  629.0 24.7 reduce-scatter.7
where the time goes:
time: 670 us; the launch traced here: 669 us
  waiting for transfers between devices  536 us (80%)
  blocking collectives  56.8 us (8%)
  matrix products  37.3 us (6%)
  other arithmetic  16.5 us (2%)
  between operations  14.8 us (2%)
  local copies, waits for them, and re-layouts  7.65 us (1%)
    all_gather x1, waiting for transfers between devices, shards(): kept_down = lax.all_gather(down_low, 'fs', axis=1, tiled=True)  93.2 us
    all_gather x1, waiting for transfers between devices, shards(): lax.all_gather(up_low, 'fs', axis=0, tiled=True)  87.9 us
    all_gather x1, waiting for transfers between devices, shards(): lax.all_gather(gate_low, 'fs', axis=0, tiled=True)  68.3 us
    reduce_scatter x3, waiting for transfers between devices, spread_back(): lax.psum_scatter(lax.dot_general(weight_cols, left_rows, (((0,), (1,)), (...  65.6 us
    all_gather x1, waiting for transfers between devices, shards(): lax.all_gather(mixout_weight.astype(jnp.bfloat16), 'fs', axis=1, tiled=True)  50.8 us
    all_gather x1, waiting for transfers between devices, shards(): lax.all_gather(value_weight.astype(jnp.bfloat16), 'fs', axis=0, tiled=True)  48.5 us
    all_gather x1, waiting for transfers between devices, shards(): lax.all_gather(bgate_low, 'fs', axis=0, tiled=True)  47.3 us
    unnamed x1, blocking collectives  39.5 us
  transfers between devices with their start and end apart: 13, of which 12 were waited for; matrix products, arithmetic and copies ran while one was open for 4% of the time, Pallas kernels for 0%

commit v1 on v0

--- a/solution.py
+++ b/solution.py
@@ -94,7 +94,12 @@
         lax.all_gather(gate_low, "fs", axis=0, tiled=True),
         lax.all_gather(up_low, "fs", axis=0, tiled=True),
     )
-    kept_down = lax.all_gather(down_low, "fs", axis=1, tiled=True)
+    ring = [down_low]
+    for hop in range(7):
+        ring.append(lax.ppermute(ring[-1], "fs", [(dev, (dev + 1) % 8) for dev in range(8)]))
+    kept_down = jnp.roll(
+        jnp.concatenate(ring[::-1], axis=1), (lax.axis_index("fs") + 1) * ring[0].shape[1], axis=1
+    )
 
     def channel_mix(gathered):
         gate_sum = jnp.dot(gathered, kept_gate, preferred_element_type=jnp.float32)

time: 670 us -> 648 us (0.967)
  waiting for transfers between devices: 536 us -> 461 us
  local copies, waits for them, and re-layouts: 7.65 us -> 31.4 us
  blocking collectives: 56.8 us -> 78.6 us
    ppermute x0 -> x7, waiting for transfers between devices: none -> 169 us  [shards(): lax.ppermute(ring[-1], 'fs', [(dev, (dev + 1) % 8) for dev in range(8)])]
    all_gather x1 -> x0, waiting for transfers between devices: 93.2 us -> none  [shards(): kept_down = lax.all_gather(down_low, 'fs', axis=1, tiled=True)]
    all_gather x1, waiting for transfers between devices: 87.9 us -> 5.47 us  [shards(): lax.all_gather(up_low, 'fs', axis=0, tiled=True)]
    all_gather x1, waiting for transfers between devices: 68.3 us -> 0.01 us  [shards(): lax.all_gather(gate_low, 'fs', axis=0, tiled=True)]
    unnamed x55 -> x76, local copies, waits for them, and re-layouts: 2.14 us -> 25.1 us
    unnamed x1, blocking collectives: 39.5 us -> 61.3 us
  transfers between devices with their start and end apart: 13 -> 19, of which waited for: 12 -> 16; matrix products, arithmetic and copies ran while one was open for 4% -> 8% of each run, Pallas kernels for 0% -> 0%
where the time goes in v1:
time: 648 us; the launch traced here: 647 us
  waiting for transfers between devices  461 us (71%)
  blocking collectives  78.6 us (12%)
  matrix products  39.5 us (6%)
  local copies, waits for them, and re-layouts  31.4 us (5%)
  other arithmetic  18.3 us (3%)
  between operations  15.1 us (2%)
    ppermute x7, waiting for transfers between devices, shards(): lax.ppermute(ring[-1], 'fs', [(dev, (dev + 1) % 8) for dev in range(8)])  169 us
    reduce_scatter x3, waiting for transfers between devices, spread_back(): lax.psum_scatter(lax.dot_general(weight_cols, left_rows, (((0,), (1,)), (...  65.6 us
    unnamed x1, blocking collectives  61.3 us
    all_gather x1, waiting for transfers between devices, shards(): lax.all_gather(mixout_weight.astype(jnp.bfloat16), 'fs', axis=1, tiled=True)  51 us
    all_gather x1, waiting for transfers between devices, shards(): lax.all_gather(value_weight.astype(jnp.bfloat16), 'fs', axis=0, tiled=True)  48.5 us
    all_gather x1, waiting for transfers between devices, shards(): lax.all_gather(bgate_low, 'fs', axis=0, tiled=True)  46.9 us
    all_gather x1, waiting for transfers between devices, shards(): lax.all_gather(cgate_weight.astype(jnp.bfloat16), 'fs', axis=0, tiled=True)  38.6 us
    all_gather x3, waiting for transfers between devices, features(): return lax.all_gather(inputs, 'tp', axis=1, tiled=True)  34.1 us
  transfers between devices with their start and end apart: 19, of which 16 were waited for; matrix products, arithmetic and copies ran while one was open for 8% of the time, Pallas kernels for 0%

profile of v1, /device:TPU:0, one launch (start us, length us, event | category | flops | bytes accessed | tf_op | source)
XLA Modules:
  0.0 647.3 jit_solution(454245976178435187)
XLA Ops:
  15.3 18.1 %collective-permute-done = bf16[1408,256]{1,0:T(8,128)(2,1)S(1)} collective-permute-done((bf16[1408,256]{1,0:T(8,128)(2,1)S(1)}, bf16[1408,256]{1,0:T(8,128)(2,1)S(1)}, u32[]{:S(2)}, u32[]{:S(2)}) %collective-permute-start) | collective-permute-done | bytes 720928 | tf_op jit(solution)/shard_map/ppermute | solution.py:99
  33.4 30.5 %collective-permute-done.1 = bf16[1408,256]{1,0:T(8,128)(2,1)S(1)} collective-permute-done((bf16[1408,256]{1,0:T(8,128)(2,1)S(1)}, bf16[1408,256]{1,0:T(8,128)(2,1)S(1)}, u32[]{:S(2)}, u32[]{:S(2)}) %collective-permute-start.1) | collective-permute-done | bytes 720928 | tf_op jit(solution)/shard_map/ppermute | solution.py:99
  63.9 28.2 %collective-permute-done.2 = bf16[1408,256]{1,0:T(8,128)(2,1)S(1)} collective-permute-done((bf16[1408,256]{1,0:T(8,128)(2,1)S(1)}, bf16[1408,256]{1,0:T(8,128)(2,1)S(1)}, u32[]{:S(2)}, u32[]{:S(2)}) %collective-permute-start.2) | collective-permute-done | bytes 720928 | tf_op jit(solution)/shard_map/ppermute | solution.py:99
  93.0 36.2 %collective-permute-done.3 = bf16[1408,256]{1,0:T(8,128)(2,1)S(1)} collective-permute-done((bf16[1408,256]{1,0:T(8,128)(2,1)S(1)}, bf16[1408,256]{1,0:T(8,128)(2,1)S(1)}, u32[]{:S(2)}, u32[]{:S(2)}) %collective-permute-start.3) | collective-permute-done | bytes 720928 | tf_op jit(solution)/shard_map/ppermute | solution.py:99
  130.1 36.1 %collective-permute-done.4 = bf16[1408,256]{1,0:T(8,128)(2,1)} collective-permute-done((bf16[1408,256]{1,0:T(8,128)(2,1)S(1)}, bf16[1408,256]{1,0:T(8,128)(2,1)}, u32[]{:S(2)}, u32[]{:S(2)}) %collective-permute-start.4) | collective-permute-done | bytes 720928 | tf_op jit(solution)/shard_map/ppermute | solution.py:99
  167.5 20.3 %collective-permute-done.5 = bf16[1408,256]{1,0:T(8,128)(2,1)} collective-permute-done((bf16[1408,256]{1,0:T(8,128)(2,1)}, bf16[1408,256]{1,0:T(8,128)(2,1)}, u32[]{:S(2)}, u32[]{:S(2)}) %collective-permute-start.5) | collective-permute-done | bytes 720928 | tf_op jit(solution)/shard_map/ppermute | solution.py:99
  189.5 61.3 %all-reduce.8 = (f32[1408]{0:T(1024)S(1)}, f32[1408]{0:T(1024)S(1)}, f32[512]{0:T(512)S(1)}, f32[512]{0:T(512)S(1)}, f32[512]{0:T(512)S(1)}, /*index=5*/f32[512]{0:T(512)S(1)}, f32[512]{0:T(512)S(1)}) all-reduce(f32[1408]{0:T(1024)S(1)} %dynamic-update-slice, f32[1408]{0:T(1024)S(1)} %dynamic-update-slice.1, ...), channel_id=1, replica_groups=mesh['fs'=8,'tp'=4] {'fs'}, use_global_device_ids=true, to_apply=%add.1 | all-reduce | flops 5376 | bytes 43008
  274.4 5.9 convolution_multiply_fusion.3
  280.3 5.5 all-gather.14.cloned.1.call-done
  285.8 9.6 %fusion.6 = bf16[2048,256]{1,0:T(8,128)(2,1)} fusion(bf16[1408,4096]{1,0:T(8,128)(2,1)} %constant_dynamic-update-slice_fusion, s32[]{:T(128)S(6)} %select_n.23, bf16[256,2048]{1,0:T(8,128)(2,1)} %all-gather.10.cloned.1.call-done, bf16[2048,1408]{1,0:T(8,128)(2,1)} %all-gather.14.cloned.1.call-done, f32[256,1408]{1,0:T(8,128)} %convolution_multiply_fusion.3, ...), kind=kOutput, calls=%fused_computation.11 | convolution fusion | flops 2955837440 | bytes 15078916 | tf_op jit(solution)/shard_map/dot_general | solution.py:36
  297.9 20.7 %reduce-scatter.4.cloned.1.call-done = bf16[512,256]{1,0:T(8,128)(2,1)} async-done(((bf16[2048,256]{1,0:T(8,128)(2,1)}), bf16[512,256]{1,0:T(8,128)(2,1)}) %reduce-scatter.4.cloned.1.call-update) | async-done | bytes 262160 | tf_op jit(solution)/shard_map/reduce_scatter | solution.py:35
  319.8 5.8 all-reduce.11
  331.1 38.6 %all-gather.20.cloned.1.call-done = bf16[2048,512]{1,0:T(8,128)(2,1)} async-done(((bf16[256,512]{1,0:T(8,128)(2,1)}), bf16[2048,512]{1,0:T(8,128)(2,1)}) %all-gather.20.cloned.1.call-update) | async-done | bytes 2097168 | tf_op jit(solution)/shard_map/all_gather | solution.py:118
  369.7 16.7 %all-gather.16.cloned.1.call-done = bf16[256,2048]{0,1:T(8,128)(2,1)} async-done(((bf16[256,512]{0,1:T(8,128)(2,1)}), bf16[256,2048]{0,1:T(8,128)(2,1)}) %all-gather.16.cloned.1.call-update) | async-done | bytes 1048592 | tf_op jit(solution)/shard_map/all_gather | solution.py:18
  389.1 48.5 %all-gather.22.cloned.1.call-done = bf16[2048,512]{1,0:T(8,128)(2,1)} async-done(((bf16[256,512]{1,0:T(8,128)(2,1)}), bf16[2048,512]{1,0:T(8,128)(2,1)}) %all-gather.22.cloned.1.call-update) | async-done | bytes 2097168 | tf_op jit(solution)/shard_map/all_gather | solution.py:121
  440.5 46.9 %all-gather.18.cloned.1.call-done = bf16[2048,512]{1,0:T(8,128)(2,1)} async-done(((bf16[256,512]{1,0:T(8,128)(2,1)}), bf16[2048,512]{1,0:T(8,128)(2,1)}) %all-gather.18.cloned.1.call-update) | async-done | bytes 2097168 | tf_op jit(solution)/shard_map/all_gather | solution.py:116
  487.4 51.0 %all-gather.24.cloned.1.call-done = bf16[512,2048]{1,0:T(8,128)(2,1)} async-done(((bf16[512,256]{1,0:T(8,128)(2,1)}), bf16[512,2048]{1,0:T(8,128)(2,1)}) %all-gather.24.cloned.1.call-update) | async-done | bytes 2097168 | tf_op jit(solution)/shard_map/all_gather | solution.py:130
  544.6 21.5 %reduce-scatter.6.cloned.1.call-done = bf16[512,256]{1,0:T(8,128)(2,1)} async-done(((bf16[2048,256]{1,0:T(8,128)(2,1)}), bf16[512,256]{1,0:T(8,128)(2,1)}) %reduce-scatter.6.cloned.1.call-update) | async-done | bytes 262160 | tf_op jit(solution)/shard_map/reduce_scatter | solution.py:35
  567.3 5.8 all-reduce.10
  575.1 17.4 %all-gather.26.cloned.1.call-done = bf16[256,2048]{0,1:T(8,128)(2,1)} async-done(((bf16[256,512]{0,1:T(8,128)(2,1)}), bf16[256,2048]{0,1:T(8,128)(2,1)}) %all-gather.26.cloned.1.call-update) | async-done | bytes 1048592 | tf_op jit(solution)/shard_map/all_gather | solution.py:18
  592.5 4.9 convolution_multiply_fusion.1
  597.4 9.1 %fusion.9 = bf16[2048,256]{1,0:T(8,128)(2,1)} fusion(bf16[1408,4096]{1,0:T(8,128)(2,1)} %constant_dynamic-update-slice_fusion, s32[]{:T(128)S(6)} %select_n.23, bf16[256,2048]{0,1:T(8,128)(2,1)S(1)} %copy-done.3, bf16[2048,1408]{1,0:T(8,128)(2,1)} %all-gather.14.cloned.1.call-done, f32[256,1408]{1,0:T(8,128)S(1)} %convolution_multiply_fusion.1, ...), kind=kOutput, calls=%fused_computation.12 | convolution fusion | flops 2955837440 | bytes 15078916 | tf_op jit(solution)/shard_map/dot_general | solution.py:36
  608.0 23.4 %reduce-scatter.8.cloned.1.call-done = bf16[512,256]{1,0:T(8,128)(2,1)} async-done(((bf16[2048,256]{1,0:T(8,128)(2,1)}), bf16[512,256]{1,0:T(8,128)(2,1)}) %reduce-scatter.8.cloned.1.call-update) | async-done | bytes 262160 | tf_op jit(solution)/shard_map/reduce_scatter | solution.py:35
  632.6 5.8 all-reduce.9
  (140 shorter events, 64.4 us)
Async XLA Ops:
  6.5 182.4 %copy-start.15 = (f32[1,176]{1,0:T(1,128)S(1)}, f32[1,176]{1,0:T(1,128)}, u32[]{:S(2)}) copy-start(f32[1,176]{1,0:T(1,128)} %param.27) | copy-start | bytes 2116
  6.6 182.6 %copy-start.19 = (f32[1,64]{1,0:T(1,128)S(1)}, f32[1,64]{1,0:T(1,128)}, u32[]{:S(2)}) copy-start(f32[1,64]{1,0:T(1,128)} %param.33) | copy-start | bytes 772
  6.6 182.7 %copy-start.20 = (f32[1,64]{1,0:T(1,128)S(1)}, f32[1,64]{1,0:T(1,128)}, u32[]{:S(2)}) copy-start(f32[1,64]{1,0:T(1,128)} %param.32) | copy-start | bytes 772
  6.6 182.8 %copy-start.21 = (f32[1,64]{1,0:T(1,128)S(1)}, f32[1,64]{1,0:T(1,128)}, u32[]{:S(2)}) copy-start(f32[1,64]{1,0:T(1,128)} %param.28) | copy-start | bytes 772
  6.6 267.8 %all-gather.10.cloned.1.call-start = ((), (), s32[]{:S(2)}) async-start(), calls=%async_computation.3 | async-start | bytes 1310720 | tf_op jit(solution)/shard_map/all_gather | solution.py:18
  7.3 267.1 %all-gather.12.cloned.1.call-start = ((), (), s32[]{:S(2)}) async-start(), calls=%async_computation.4 | async-start | bytes 6488064 | tf_op jit(solution)/shard_map/all_gather | solution.py:94
  9.7 276.1 %all-gather.14.cloned.1.call-start = ((), (), s32[]{:S(2)}) async-start(), calls=%async_computation.5 | async-start | bytes 6488064 | tf_op jit(solution)/shard_map/all_gather | solution.py:95
  11.2 22.2 %collective-permute-start = (bf16[1408,256]{1,0:T(8,128)(2,1)S(1)}, bf16[1408,256]{1,0:T(8,128)(2,1)S(1)}, u32[]{:S(2)}, u32[]{:S(2)}) collective-permute-start(bf16[1408,256]{1,0:T(8,128)(2,1)S(1)} %convert_element_type.72), channel_id=1, source_target_pairs={{0,4},{4,8},{8,12},{12,16},{16,20},{20,24},{24,28},{28,0},{1,5},{5... | collective-permute-start | bytes 2162696 | tf_op jit(solution)/shard_map/ppermute | solution.py:99
  15.2 247.0 %copy-start = (f32[1408,256]{1,0:T(8,128)S(1)}, f32[1408,256]{1,0:T(8,128)}, u32[]{:S(2)}) copy-start(f32[1408,256]{1,0:T(8,128)} %param.25) | copy-start | bytes 4325380
  15.2 303.4 %reduce-scatter.4.cloned.1.call-start = ((), (), s32[]{:S(2)}) async-start(), calls=%async_computation.6 | async-start | bytes 1310720 | tf_op jit(solution)/shard_map/reduce_scatter | solution.py:35
  33.4 30.5 %collective-permute-start.1 = (bf16[1408,256]{1,0:T(8,128)(2,1)S(1)}, bf16[1408,256]{1,0:T(8,128)(2,1)S(1)}, u32[]{:S(2)}, u32[]{:S(2)}) collective-permute-start(bf16[1408,256]{1,0:T(8,128)(2,1)S(1)} %collective-permute-done), channel_id=1, source_target_pairs={{0,4},{4,8},{8,12},{12,16},{16,20},{20,24},{24,28},{28,0},{1,5},{5... | collective-permute-start | bytes 2162696 | tf_op jit(solution)/shard_map/ppermute | solution.py:99
  63.9 28.2 %collective-permute-start.2 = (bf16[1408,256]{1,0:T(8,128)(2,1)S(1)}, bf16[1408,256]{1,0:T(8,128)(2,1)S(1)}, u32[]{:S(2)}, u32[]{:S(2)}) collective-permute-start(bf16[1408,256]{1,0:T(8,128)(2,1)S(1)} %collective-permute-done.1), channel_id=1, source_target_pairs={{0,4},{4,8},{8,12},{12,16},{16,20},{20,24},{24,28},{28,0},{1,5},{5... | collective-permute-start | bytes 2162696 | tf_op jit(solution)/shard_map/ppermute | solution.py:99
  93.0 36.2 %collective-permute-start.3 = (bf16[1408,256]{1,0:T(8,128)(2,1)S(1)}, bf16[1408,256]{1,0:T(8,128)(2,1)S(1)}, u32[]{:S(2)}, u32[]{:S(2)}) collective-permute-start(bf16[1408,256]{1,0:T(8,128)(2,1)S(1)} %collective-permute-done.2), channel_id=1, source_target_pairs={{0,4},{4,8},{8,12},{12,16},{16,20},{20,24},{24,28},{28,0},{1,5},{5... | collective-permute-start | bytes 2162696 | tf_op jit(solution)/shard_map/ppermute | solution.py:99
  130.1 36.1 %collective-permute-start.4 = (bf16[1408,256]{1,0:T(8,128)(2,1)S(1)}, bf16[1408,256]{1,0:T(8,128)(2,1)}, u32[]{:S(2)}, u32[]{:S(2)}) collective-permute-start(bf16[1408,256]{1,0:T(8,128)(2,1)S(1)} %collective-permute-done.3), channel_id=1, source_target_pairs={{0,4},{4,8},{8,12},{12,16},{16,20},{20,24},{24,28},{28,0},{1,5},{5... | collective-permute-start | bytes 2162696 | tf_op jit(solution)/shard_map/ppermute | solution.py:99
  166.2 21.7 %collective-permute-start.5 = (bf16[1408,256]{1,0:T(8,128)(2,1)}, bf16[1408,256]{1,0:T(8,128)(2,1)}, u32[]{:S(2)}, u32[]{:S(2)}) collective-permute-start(bf16[1408,256]{1,0:T(8,128)(2,1)} %collective-permute-done.4), channel_id=1, source_target_pairs={{0,4},{4,8},{8,12},{12,16},{16,20},{20,24},{24,28},{28,0},{1,5},{5... | collective-permute-start | bytes 2162696 | tf_op jit(solution)/shard_map/ppermute | solution.py:99
  187.8 63.0 %collective-permute-start.6 = (bf16[1408,256]{1,0:T(8,128)(2,1)}, bf16[1408,256]{1,0:T(8,128)(2,1)}, u32[]{:S(2)}, u32[]{:S(2)}) collective-permute-start(bf16[1408,256]{1,0:T(8,128)(2,1)} %collective-permute-done.5), channel_id=1, source_target_pairs={{0,4},{4,8},{8,12},{12,16},{16,20},{20,24},{24,28},{28,0},{1,5},{5... | collective-permute-start | bytes 2162696 | tf_op jit(solution)/shard_map/ppermute | solution.py:99
  295.4 74.3 %all-gather.20.cloned.1.call-start = ((), (), s32[]{:S(2)}) async-start(), calls=%async_computation.9 | async-start | bytes 2359296 | tf_op jit(solution)/shard_map/all_gather | solution.py:118
  296.2 90.2 %all-gather.16.cloned.1.call-start = ((), (), s32[]{:S(2)}) async-start(), calls=%async_computation.7 | async-start | bytes 1310720 | tf_op jit(solution)/shard_map/all_gather | solution.py:18
  327.5 110.1 %all-gather.22.cloned.1.call-start = ((), (), s32[]{:S(2)}) async-start(), calls=%async_computation.10 | async-start | bytes 2359296 | tf_op jit(solution)/shard_map/all_gather | solution.py:121
  328.3 159.1 %all-gather.18.cloned.1.call-start = ((), (), s32[]{:S(2)}) async-start(), calls=%async_computation.8 | async-start | bytes 2359296 | tf_op jit(solution)/shard_map/all_gather | solution.py:116
  329.1 209.2 %all-gather.24.cloned.1.call-start = ((), (), s32[]{:S(2)}) async-start(), calls=%async_computation.11 | async-start | bytes 2359296 | tf_op jit(solution)/shard_map/all_gather | solution.py:130
  329.9 236.2 %reduce-scatter.6.cloned.1.call-start = ((), (), s32[]{:S(2)}) async-start(), calls=%async_computation.12 | async-start | bytes 1310720 | tf_op jit(solution)/shard_map/reduce_scatter | solution.py:35
  543.0 49.5 %all-gather.26.cloned.1.call-start = ((), (), s32[]{:S(2)}) async-start(), calls=%async_computation.13 | async-start | bytes 1310720 | tf_op jit(solution)/shard_map/all_gather | solution.py:18
  575.0 56.4 %reduce-scatter.8.cloned.1.call-start = ((), (), s32[]{:S(2)}) async-start(), calls=%async_computation.14 | async-start | bytes 1310720 | tf_op jit(solution)/shard_map/reduce_scatter | solution.py:35
  (18 other events, 1169.9 us)
Sparse Core Ops, SparseCore 0:
  9.0 19.4 all-gather.9
  30.6 133.5 all-gather.11
  166.4 119.2 all-gather.13
  295.5 23.0 reduce-scatter.3
  320.6 49.0 all-gather.19
  371.1 15.2 all-gather.15
  388.5 49.0 all-gather.21
  439.7 47.6 all-gather.17
  489.4 48.8 all-gather.23
  543.1 22.9 reduce-scatter.5
  575.1 17.3 all-gather.25
  606.6 24.7 reduce-scatter.7
